TPU v7x, 32 devices: a whole 2x2x4 slice. The times are simulated.
32 devices in a mesh: ep: 8 (over z, core), tp: 4 (over y, x).
Axes of the slice: x: 2, y: 2, z: 4, core: 2. Of those that a mesh axis runs over, the one named last changes fastest.
Arguments:
- tokens: bfloat16 [128, 4096], P('ep', 'tp'), may hold values from -40 to 40
- routes: int32 [128, 4], P('ep'), may hold values from 0 to 15, all different within a row; in each aligned block of 16 rows (0 to 15, 16 to 31, ...) at most 6 rows name the same one
- gates: float32 [128, 4], P('ep'), may hold values from 0.1 to 1
- pre_gain: bfloat16 [4096], P('tp'), may hold values from 0.099609375 to 1.8984375
- expert_gate: bfloat16 [16, 4096, 1024], P('ep', 'tp'), may hold values from -0.09375 to 0.09375
- expert_up: bfloat16 [16, 4096, 1024], P('ep', 'tp'), may hold values from -0.09375 to 0.09375
- expert_down: bfloat16 [16, 1024, 4096], P('ep', None, 'tp'), may hold values from -0.125 to 0.125
- shared_gate: bfloat16 [4096, 1024], P('tp'), may hold values from -0.09375 to 0.09375
- shared_up: bfloat16 [4096, 1024], P('tp'), may hold values from -0.09375 to 0.09375
- shared_down: bfloat16 [1024, 4096], P(None, 'tp'), may hold values from -0.125 to 0.125
- out_gain: bfloat16 [4096], P('tp'), may hold values from 0.099609375 to 1.8984375
Outputs:
- mixed: bfloat16 [128, 4096], P('ep', 'tp')
Inputs may be any that keep to these rules, and one draw needn't show every extreme that they name: `routes`: each row names 4 different experts, and expert e is held by index e // 2 of ep. Among the 16 rows of one index of ep no expert is named by more than 6 rows, and in every draw some expert is named by exactly 6 rows of some index.
All inputs are finite; a program needn't handle non-finite values.
Results may differ from a plain program's by a relative error of at most 0.012.
Values may be sent and summed in bfloat16 or wider, within the bound.
A program may use at most 64 MiB of HBM per device.

v0:
```python
import functools
import jax
import jax.numpy as jnp
from jax import lax
from jax.experimental import pallas as pl
from jax.experimental.pallas import tpu as pltpu
from jax.sharding import PartitionSpec as P

D = 4096


def normalize(values, gain, squares, width):
    scale = lax.rsqrt(squares[:, None] / width + 1e-06)
    return values * scale * gain.astype(jnp.float32)


def expert_apply(buffer, expert_gate, expert_up, expert_down, shared_gate_part, shared_up_part):
    gate_part = jnp.einsum(
        "secd,edf->secf", buffer, expert_gate, preferred_element_type=jnp.float32
    )
    up_part = jnp.einsum("secd,edf->secf", buffer, expert_up, preferred_element_type=jnp.float32)
    gate_act, up_act, shared_gate_act, shared_up_act = lax.psum(
        (gate_part, up_part, shared_gate_part, shared_up_part), "tp"
    )
    hidden = (jax.nn.silu(gate_act) * up_act).astype(jnp.bfloat16)
    shared_hidden = (jax.nn.silu(shared_gate_act) * shared_up_act).astype(jnp.bfloat16)
    results = jnp.einsum(
        "secf,efd->secd", hidden, expert_down, preferred_element_type=jnp.float32
    ).astype(jnp.bfloat16)
    return (results, shared_hidden)


def on_device(
    tokens,
    routes,
    gates,
    pre_gain,
    expert_gate,
    expert_up,
    expert_down,
    shared_gate,
    shared_up,
    shared_down,
    out_gain,
):
    own_rows = tokens.astype(jnp.float32)
    in_squares = lax.psum(jnp.sum(own_rows * own_rows, axis=1), "tp")
    normed = normalize(own_rows, pre_gain, in_squares, D).astype(jnp.bfloat16)
    shared_gate_part = jnp.dot(normed, shared_gate, preferred_element_type=jnp.float32)
    shared_up_part = jnp.dot(normed, shared_up, preferred_element_type=jnp.float32)
    tok_count = tokens.shape[0]
    top_count = routes.shape[1]
    groups = lax.axis_size("ep")
    local_experts = expert_gate.shape[0]
    experts_all = local_experts * groups
    capacity = max(2, 3 * tok_count * top_count // (2 * experts_all))
    places = jnp.arange(capacity, dtype=jnp.int32)
    zero_value = jnp.zeros((), jnp.float32)
    labels = jnp.arange(experts_all, dtype=jnp.int32)
    picked = routes[:, :, None] == labels[None, None, :]
    onehot = jnp.sum(picked.astype(jnp.int32), axis=1)
    dense_gate = jnp.sum(jnp.where(picked, gates[:, :, None], zero_value), axis=1)
    slot_index = jnp.cumsum(onehot, axis=0) - onehot
    select = (slot_index.T[:, None, :] == places[None, :, None]) & (onehot.T[:, None, :] > 0)
    outgoing = jnp.einsum(
        "ect,td->ecd", select.astype(jnp.bfloat16), normed, preferred_element_type=jnp.float32
    ).astype(jnp.bfloat16)
    outgoing = outgoing.reshape(groups, local_experts, capacity, normed.shape[1])
    received = lax.all_to_all(outgoing, "ep", split_axis=0, concat_axis=0, tiled=True)
    results, shared_hidden = expert_apply(
        received, expert_gate, expert_up, expert_down, shared_gate_part, shared_up_part
    )
    returned = lax.all_to_all(results, "ep", split_axis=0, concat_axis=0, tiled=True)
    weight = jnp.where(select, dense_gate.T[:, None, :], zero_value)
    returned_rows = returned.reshape(experts_all, capacity, normed.shape[1]).astype(jnp.float32)
    routed = jnp.einsum("ect,ecd->td", weight, returned_rows, precision=lax.Precision.HIGHEST)
    shared_out = jnp.dot(shared_hidden, shared_down, preferred_element_type=jnp.float32)
    combined = routed + shared_out
    out_squares = lax.psum(jnp.sum(combined * combined, axis=1), "tp")
    return normalize(combined, out_gain, out_squares, D).astype(jnp.bfloat16)


F32 = jnp.float32
BF16 = jnp.bfloat16
LANES = 128


def flip(index, mask):
    out, bit = index, 1
    while bit <= mask:
        if mask & bit:
            out = out + bit - 2 * bit * ((index // bit) % 2)
        bit *= 2
    return out


def iota(shape, dim):
    return lax.broadcasted_iota(jnp.int32, shape, dim)


def dot(a, b):
    return jnp.dot(a, b, preferred_element_type=F32)


def fused_kernel(
    n_ep, n_tp, cap, width,
    tok_hbm, routes_hbm, gates_hbm, pre_hbm, eg_hbm, eu_hbm, ed_hbm, sg_hbm, su_hbm, sd_hbm, outg_hbm,
    o_ref,
    tok_ref, routes_ref, gates_ref, pre_ref, outg_ref,
    wg, wu, wd, sg, su, sd,
    xall, ss_all, buf,
    rs_send, rs_recv, rs_own, rsh_send, rsh_recv, rsh_own,
    hid, hidsh, acc, yown, ysend, yhold, ypair, zsend, zrecv, sq_all,
    w_sem, x_send, x_recv, f_send, f_recv, ss_send, ss_recv, rs_ssem, rs_rsem, rsh_ssem, rsh_rsem,
    h_ssem, h_rsem, hs_ssem, hs_rsem, p_ssem, p_rsem, y_ssem, y_rsem, q_ssem, q_rsem,
):
    me = lax.axis_index("ep")
    mine = lax.axis_index("tp")
    tok, dim = tok_ref.shape
    local = eg_hbm.shape[0]
    experts = local * n_ep
    top = routes_hbm.shape[0]
    per = n_ep * cap
    rows = local * per
    hidden = eg_hbm.shape[2]
    part = hidden // n_tp
    total = n_ep * tok
    far = list(range(2, n_ep, 2))
    tp_masks = sorted(range(1, n_tp), key=lambda m: -bin(m).count("1"))
    pending = []

    def at_ep(mask):
        return {"ep": flip(me, mask)}

    def at_tp(mask):
        return {"tp": flip(mine, mask)}

    barrier = pltpu.get_barrier_semaphore()
    for m in far + [1]:
        pl.semaphore_signal(barrier, inc=1, device_id=at_ep(m), device_id_type=pl.DeviceIdType.MESH)
    for m in range(1, n_tp):
        pl.semaphore_signal(barrier, inc=1, device_id=at_tp(m), device_id_type=pl.DeviceIdType.MESH)

    copies = {}

    def fetch(name, src, dst, index):
        copies[name] = pltpu.make_async_copy(src, dst, w_sem.at[index])
        copies[name].start()

    small = 3 + 3 * local
    fetch("routes", routes_hbm, routes_ref, small)
    fetch("gates", gates_hbm, gates_ref, small + 1)
    fetch("tok", tok_hbm, tok_ref, small + 2)
    fetch("pre", pre_hbm, pre_ref, small + 3)
    fetch("outg", outg_hbm, outg_ref, small + 4)
    fetch("sg", sg_hbm, sg, 0)
    fetch("su", su_hbm, su, 1)
    for e in range(local):
        fetch(("g", e), eg_hbm.at[e], wg.at[e], 3 + e)
        fetch(("u", e), eu_hbm.at[e], wu.at[e], 3 + local + e)
    fetch("sd", sd_hbm, sd, 2)
    for e in range(local):
        fetch(("d", e), ed_hbm.at[e], wd.at[e], 3 + 2 * local + e)

    def send(src, dst, ssem, rsem, where):
        copy = pltpu.make_async_remote_copy(
            src_ref=src, dst_ref=dst, send_sem=ssem, recv_sem=rsem,
            device_id=where, device_id_type=pl.DeviceIdType.MESH,
        )
        copy.start()
        pending.append(copy)
        return copy

    def flat_gain(ref):
        value = ref[...].astype(F32)
        return jnp.concatenate([value[i : i + 1, :] for i in range(ref.shape[0])], axis=1)

    copies["routes"].wait()
    copies["gates"].wait()
    row = iota((LANES, tok), 0)
    names = row % experts
    dense = jnp.zeros((LANES, tok), F32)
    for k in range(top):
        dense = dense + jnp.where(routes_ref[k : k + 1, :] == names, gates_ref[k : k + 1, :], 0.0)
    earlier = jnp.where(iota((tok, tok), 0) < iota((tok, tok), 1), 1.0, 0.0).astype(BF16)
    slots = dot(jnp.where(dense > 0.0, 1.0, 0.0).astype(BF16), earlier)
    slots = jnp.where(dense > 0.0, slots + 1.0, 0.0)

    def terms(value):
        hi = value.astype(BF16).astype(F32)
        mid = (value - hi).astype(BF16).astype(F32)
        return hi, mid, value - hi - mid

    def choose(index, values):
        out = 0.0
        for i, value in enumerate(values):
            out = jnp.where(index == i, value, out)
        return out

    listed = choose(row // experts, terms(dense) + (slots,)).astype(BF16)
    eye = jnp.where(iota((tok, tok), 0) == iota((tok, tok), 1), 1.0, 0.0).astype(BF16)
    meta = lax.dot_general(eye, listed, (((1,), (1,)), ((), ())), preferred_element_type=F32)
    copies["tok"].wait()
    copies["pre"].wait()
    x = tok_ref[...].astype(F32)
    xall[me, :, :dim] = (x * flat_gain(pre_ref)).astype(BF16)
    squares = jnp.sum(x * x, axis=1, keepdims=True)
    lane = iota((tok, LANES), 1)
    meta = jnp.where(lane < 4 * experts, meta, choose(lane - 4 * experts, terms(squares)))
    xall[me, :, dim:] = meta.astype(BF16)

    pl.semaphore_wait(barrier, len(far) + 1 + n_tp - 1)

    own_block = xall.at[me]
    got = {}
    for m in far + [1]:
        got[m] = send(own_block, own_block, x_send.at[m], x_recv.at[m], at_ep(m))

    xs = xall[me, :, :dim]
    copies["sg"].wait()
    copies["su"].wait()
    shared_in = {}
    for m in tp_masks + [0]:
        cols = pl.ds(pl.multiple_of(flip(mine, m) * part, part), part)
        g = dot(xs, sg[:, cols])
        u = dot(xs, su[:, cols])
        if m:
            rsh_send[m - 1, :, :part] = g.astype(BF16)
            rsh_send[m - 1, :, part:] = u.astype(BF16)
            shared_in[m] = send(rsh_send.at[m - 1], rsh_recv.at[m - 1], rsh_ssem.at[m], rsh_rsem.at[m], at_tp(m))
        else:
            rsh_own[:, :part] = g
            rsh_own[:, part:] = u

    relayed = []
    for m in far:
        got[m].wait_recv()
        block = xall.at[flip(me, m)]
        relayed.append(send(block, block, f_send.at[m], f_recv.at[m], at_ep(1)))
    got[1].wait_recv()
    for copy in relayed:
        copy.wait_recv()

    tail = xall[:, :, dim:].reshape(total, LANES)
    row8, lane8 = iota((8, LANES), 0), iota((8, LANES), 1)
    gate_lane = lane8 < 3 * experts
    slot_lane = (lane8 >= 3 * experts) & (lane8 < 4 * experts)
    mine8 = me * local + row8
    pick = (
        ((row8 < local) & gate_lane & (lane8 % experts == mine8))
        | ((row8 == local) & (lane8 >= 4 * experts))
        | ((row8 > local) & (row8 <= 2 * local) & slot_lane & (lane8 % experts == mine8 - local - 1))
    )
    table = lax.dot_general(
        jnp.where(pick, 1.0, 0.0).astype(BF16), tail, (((1,), (1,)), ((), ())), preferred_element_type=F32
    )
    ss_all[mine] = table
    ss_in = [
        send(ss_all.at[mine], ss_all.at[mine], ss_send.at[m], ss_recv.at[m], at_tp(m)) for m in tp_masks
    ]
    first = (iota((8, total), 1) // tok) * cap - 1
    target = jnp.where(table > 0.5, first + table.astype(jnp.int32), -1)
    pieces = [
        jnp.where(iota((per, total), 0) == target[local + 1 + e : local + 2 + e, :], 1.0, 0.0)
        for e in range(local)
    ]
    gate_col = jnp.concatenate(
        [jnp.sum(pieces[e] * table[e : e + 1, :], axis=1, keepdims=True) for e in range(local)], axis=0
    )
    own = jnp.where(iota((tok, total), 1) == me * tok + iota((tok, total), 0), 1.0, 0.0)
    select = jnp.concatenate(pieces, axis=0)
    chosen = select.astype(BF16)
    flat = xall[:, :, :dim].reshape(total, dim)
    buf[...] = dot(chosen, flat).astype(BF16)

    routed_in = {}
    for e in range(local):
        copies["g", e].wait()
        copies["u", e].wait()
        here = pl.ds(e * per, per)
        rhs = buf[here, :]
        for m in tp_masks + [0]:
            cols = pl.ds(pl.multiple_of(flip(mine, m) * part, part), part)
            g = dot(rhs, wg[e, :, cols])
            u = dot(rhs, wu[e, :, cols])
            if m:
                rs_send[m - 1, here, :part] = g.astype(BF16)
                rs_send[m - 1, here, part:] = u.astype(BF16)
                routed_in[m, e] = send(
                    rs_send.at[m - 1, here], rs_recv.at[m - 1, here],
                    rs_ssem.at[m * local + e], rs_rsem.at[m * local + e], at_tp(m),
                )
            else:
                rs_own[here, :part] = g
                rs_own[here, part:] = u

    for copy in ss_in:
        copy.wait_recv()
    ss = ss_all[0, local : local + 1, :]
    for q in range(1, n_tp):
        ss = ss + ss_all[q, local : local + 1, :]
    scale = lax.rsqrt(ss / width + 1e-06)
    row_scale = jnp.sum(select * scale, axis=1, keepdims=True)
    own_scale = jnp.sum(own * scale, axis=1, keepdims=True)

    def activate(sums, by):
        g, u = sums[:, :part] * by, sums[:, part:] * by
        return (g / (1.0 + jnp.exp(-g)) * u).astype(BF16)

    routed_hid, shared_hid = {}, []
    for e in range(local):
        here = pl.ds(e * per, per)
        sums = rs_own[here, :]
        for m in tp_masks:
            routed_in[m, e].wait_recv()
            sums = sums + rs_recv[m - 1, here, :].astype(F32)
        hid[mine, here, :] = activate(sums, row_scale[e * per : (e + 1) * per, :])
        for m in tp_masks:
            block = hid.at[mine, here]
            routed_hid[m, e] = send(block, block, h_ssem.at[m * local + e], h_rsem.at[m * local + e], at_tp(m))
        if e == 0:
            sums = rsh_own[...]
            for m in tp_masks:
                shared_in[m].wait_recv()
                sums = sums + rsh_recv[m - 1].astype(F32)
            hidsh[mine] = activate(sums, own_scale)
            block = hidsh.at[mine]
            shared_hid = [send(block, block, hs_ssem.at[m], hs_rsem.at[m], at_tp(m)) for m in tp_masks]

    for e in range(local):
        copies["d", e].wait()

    def down(q, e):
        piece = pl.ds(pl.multiple_of(q * part, part), part)
        return dot(hid[q, pl.ds(e * per, per), :], wd[e, piece, :])

    for e in range(local):
        acc[pl.ds(e * per, per), :] = down(mine, e)
    copies["sd"].wait()
    for copy in shared_hid:
        copy.wait_recv()
    shared_out = dot(hidsh[0], sd[0:part, :])
    for q in range(1, n_tp):
        shared_out = shared_out + dot(hidsh[q], sd[q * part : (q + 1) * part, :])
    yown[...] = shared_out
    for e in range(local):
        for m in tp_masks[::-1]:
            routed_hid[m, e].wait_recv()
            acc[pl.ds(e * per, per), :] += down(flip(mine, m), e)

    gated = (acc[...] * gate_col).astype(BF16)
    back = lax.dot_general(chosen, gated, (((0,), (0,)), ((), ())), preferred_element_type=F32)
    back = back.reshape(n_ep, tok, dim)
    ysend[...] = back.astype(BF16)
    yhold[...] = back
    paired = {}
    for m in far + [0]:
        paired[m] = send(ysend.at[flip(me, m + 1)], ypair.at[m // 2], p_ssem.at[m], p_rsem.at[m], at_ep(1))
    answers = {}
    for m in far:
        paired[m].wait_recv()
        zsend[m // 2] = (yhold[flip(me, m)] + ypair[m // 2].astype(F32)).astype(BF16)
        answers[m] = send(zsend.at[m // 2], zrecv.at[m // 2], y_ssem.at[m], y_rsem.at[m], at_ep(m))
    paired[0].wait_recv()
    combined = yown[...] + yhold[me] + ypair[0].astype(F32)
    copies["outg"].wait()
    for m in far:
        answers[m].wait_recv()
        combined = combined + zrecv[m // 2].astype(F32)

    squared = combined * combined
    lanes = squared[:, :LANES]
    for c in range(LANES, dim, LANES):
        lanes = lanes + squared[:, c : c + LANES]
    sq_all[mine] = lanes
    last = [
        send(sq_all.at[mine], sq_all.at[mine], q_ssem.at[m], q_rsem.at[m], at_tp(m)) for m in tp_masks
    ]
    scaled = combined * flat_gain(outg_ref)
    for copy in last:
        copy.wait_recv()
    lanes = sq_all[0]
    for q in range(1, n_tp):
        lanes = lanes + sq_all[q]
    mean = jnp.sum(lanes, axis=1, keepdims=True) / width
    o_ref[...] = (scaled * lax.rsqrt(mean + 1e-06)).astype(BF16)
    for copy in pending:
        copy.wait_send()


def fused(n_ep, n_tp, tokens, routes, gates, pre_gain, eg, eu, ed, sg, su, sd, out_gain):
    tok, dim = tokens.shape
    local, _, hidden = eg.shape
    top = routes.shape[1]
    cap = max(2, 3 * tok * top // (2 * local * n_ep))
    per = n_ep * cap
    rows = local * per
    part = hidden // n_tp
    vmem, anywhere = pl.BlockSpec(memory_space=pltpu.VMEM), pl.BlockSpec(memory_space=pl.ANY)
    sems = lambda n: pltpu.SemaphoreType.DMA((n,))
    return pl.pallas_call(
        functools.partial(fused_kernel, n_ep, n_tp, cap, dim * n_tp),
        out_shape=jax.ShapeDtypeStruct((tok, dim), BF16),
        in_specs=[anywhere] * 11,
        out_specs=vmem,
        scratch_shapes=[
            pltpu.VMEM((tok, dim), BF16), pltpu.VMEM((top, tok), jnp.int32), pltpu.VMEM((top, tok), F32),
            pltpu.VMEM((dim // LANES, LANES), BF16), pltpu.VMEM((dim // LANES, LANES), BF16),
            pltpu.VMEM(eg.shape, BF16), pltpu.VMEM(eu.shape, BF16), pltpu.VMEM(ed.shape, BF16),
            pltpu.VMEM(sg.shape, BF16), pltpu.VMEM(su.shape, BF16), pltpu.VMEM(sd.shape, BF16),
            pltpu.VMEM((n_ep, tok, dim + LANES), BF16),
            pltpu.VMEM((n_tp, 8, n_ep * tok), F32),
            pltpu.VMEM((rows, dim), BF16),
            pltpu.VMEM((n_tp - 1, rows, 2 * part), BF16),
            pltpu.VMEM((n_tp - 1, rows, 2 * part), BF16),
            pltpu.VMEM((rows, 2 * part), F32),
            pltpu.VMEM((n_tp - 1, tok, 2 * part), BF16),
            pltpu.VMEM((n_tp - 1, tok, 2 * part), BF16),
            pltpu.VMEM((tok, 2 * part), F32),
            pltpu.VMEM((n_tp, rows, part), BF16),
            pltpu.VMEM((n_tp, tok, part), BF16),
            pltpu.VMEM((rows, dim), F32),
            pltpu.VMEM((tok, dim), F32),
            pltpu.VMEM((n_ep, tok, dim), BF16),
            pltpu.VMEM((n_ep, tok, dim), F32),
            pltpu.VMEM((n_ep // 2, tok, dim), BF16),
            pltpu.VMEM((n_ep // 2, tok, dim), BF16),
            pltpu.VMEM((n_ep // 2, tok, dim), BF16),
            pltpu.VMEM((n_tp, tok, LANES), F32),
            sems(8 + 3 * local),
            sems(n_ep), sems(n_ep), sems(n_ep), sems(n_ep),
            sems(n_tp), sems(n_tp), sems(n_tp * local), sems(n_tp * local), sems(n_tp), sems(n_tp),
            sems(n_tp * local), sems(n_tp * local), sems(n_tp), sems(n_tp),
            sems(n_ep), sems(n_ep), sems(n_ep), sems(n_ep), sems(n_tp), sems(n_tp),
        ],
        compiler_params=pltpu.CompilerParams(
            collective_id=0, has_side_effects=True, vmem_limit_bytes=60 * 1024 * 1024
        ),
    )(
        tokens, routes.T, gates.T, pre_gain.reshape(-1, LANES), eg, eu, ed, sg, su, sd,
        out_gain.reshape(-1, LANES),
    )


def fits(n_ep, n_tp, tokens, routes, eg):
    tok, dim = tokens.shape
    local, _, hidden = eg.shape
    experts = local * n_ep
    cap = max(2, 3 * tok * routes.shape[1] // (2 * experts))
    power = (n_ep & (n_ep - 1)) == 0 and (n_tp & (n_tp - 1)) == 0
    return (
        power
        and n_ep > 1
        and n_tp > 1
        and hidden % (LANES * n_tp) == 0
        and dim % LANES == 0
        and tok % 16 == 0
        and (n_ep * cap) % 16 == 0
        and n_ep * tok == LANES
        and 4 * experts + 3 <= LANES
        and 2 * local < 8
        and n_ep > 2
    )


def per_device(*args):
    n_ep, n_tp = lax.axis_size("ep"), lax.axis_size("tp")
    if fits(n_ep, n_tp, args[0], args[1], args[4]):
        return fused(n_ep, n_tp, *args)
    return on_device(*args)


def solution(mesh):
    in_specs = (
        P("ep", "tp"),
        P("ep", None),
        P("ep", None),
        P("tp"),
        P("ep", "tp", None),
        P("ep", "tp", None),
        P("ep", None, "tp"),
        P("tp", None),
        P("tp", None),
        P(None, "tp"),
        P("tp"),
    )
    out_specs = P("ep", "tp")
    return jax.shard_map(
        per_device, mesh=mesh, in_specs=in_specs, out_specs=out_specs, check_vma=False
    )
```

profile of v0, /device:TPU:0, one launch (start us, length us, event | category | flops | bytes accessed | tf_op | source)
XLA Modules:
  0.0 34.7 jit_solution(9218811746599100815)
XLA Ops:
  0.0 33.3 %shard_map.109 = bf16[16,1024]{1,0:T(8,128)(2,1)} custom-call(bf16[16,1024]{1,0:T(8,128)(2,1)} %tok_hbm.1, s32[4,16]{1,0:T(4,128)} %bitcast.4, f32[4,16]{1,0:T(4,128)} %bitcast.5, bf16[8,128]{1,0:T(8,128)(2,1)} %bitcast.6, bf16[2,1024,1024]{2,1,0:T(8,128)(2,1)} %eg_hbm.1, bf16[2,1024,1024]{2,1,0:T(8,128)(2,1)} %eu_hbm.1, bf16[2,1024,1024]{2,1,0:T(8,128)(2,1)} %ed_hbm.1, ...), custom_call_target="tpu_custom_call" | custom-call | tf_op jit(solution)/shard_map/pallas_call | solution.py:401
  33.3 1.4 %copy.13 = bf16[16,1024]{1,0:T(8,128)(2,1)} copy(bf16[16,1024]{1,0:T(8,128)(2,1)} %shard_map.109) | data formatting | bytes 65536
where the time goes:
time: 34.8 us; the launch traced here: 34.7 us
  Pallas kernels  33.3 us (96%)
  local copies, waits for them, and re-layouts  1.38 us (4%)
    pallas_call x1, Pallas kernels, fused(): pl.pallas_call(functools.partial(fused_kernel, n_ep, n_tp, cap, dim * n_t...  33.3 us
    unnamed x1, local copies, waits for them, and re-layouts  1.38 us

commit v1 on v0

--- a/solution.py
+++ b/solution.py
@@ -400,7 +400,7 @@
     sems = lambda n: pltpu.SemaphoreType.DMA((n,))
     return pl.pallas_call(
         functools.partial(fused_kernel, n_ep, n_tp, cap, dim * n_tp),
-        out_shape=jax.ShapeDtypeStruct((tok, dim), BF16),
+        out_shape=pltpu.VMEM((tok, dim), BF16),
         in_specs=[anywhere] * 11,
         out_specs=vmem,
         scratch_shapes=[

time: 34.8 us -> 33.5 us (0.963)
  local copies, waits for them, and re-layouts: 1.38 us -> 0.62 us
  Pallas kernels: 33.3 us -> 32.7 us
    unnamed x1, local copies, waits for them, and re-layouts: 1.38 us -> 0.62 us
    pallas_call x1, Pallas kernels: 33.3 us -> 32.7 us  [fused(): pl.pallas_call(functools.partial(fused_kernel, n_ep, n_tp, cap, dim * n_t...]
where the time goes in v1:
time: 33.5 us; the launch traced here: 33.3 us
  Pallas kernels  32.7 us (98%)
  local copies, waits for them, and re-layouts  0.62 us (2%)
    pallas_call x1, Pallas kernels, fused(): pl.pallas_call(functools.partial(fused_kernel, n_ep, n_tp, cap, dim * n_t...  32.7 us

profile of v1, /device:TPU:0, one launch (start us, length us, event | category | flops | bytes accessed | tf_op | source)
XLA Modules:
  0.0 33.3 jit_solution(8921112174655594003)
XLA Ops:
  0.0 32.7 %shard_map.109 = bf16[16,1024]{1,0:T(8,128)(2,1)S(1)} custom-call(bf16[16,1024]{1,0:T(8,128)(2,1)} %tok_hbm.1, s32[4,16]{1,0:T(4,128)} %bitcast.4, f32[4,16]{1,0:T(4,128)} %bitcast.5, bf16[8,128]{1,0:T(8,128)(2,1)} %bitcast.6, bf16[2,1024,1024]{2,1,0:T(8,128)(2,1)} %eg_hbm.1, bf16[2,1024,1024]{2,1,0:T(8,128)(2,1)} %eu_hbm.1, bf16[2,1024,1024]{2,1,0:T(8,128)(2,1)} %ed_hbm.1, ...), custom_call_target="tpu_custom_call" | custom-call | tf_op jit(solution)/shard_map/pallas_call | solution.py:401
  32.7 0.6 %copy.13 = bf16[16,1024]{1,0:T(8,128)(2,1)} copy(bf16[16,1024]{1,0:T(8,128)(2,1)S(1)} %shard_map.109) | data formatting | bytes 65536

commit v2 on v1

v2 whole, which is shorter than its diff:
```python
import functools
import jax
import jax.numpy as jnp
from jax import lax
from jax.experimental import pallas as pl
from jax.experimental.pallas import tpu as pltpu
from jax.sharding import PartitionSpec as P

D = 4096


def normalize(values, gain, squares, width):
    scale = lax.rsqrt(squares[:, None] / width + 1e-06)
    return values * scale * gain.astype(jnp.float32)


def expert_apply(buffer, expert_gate, expert_up, expert_down, shared_gate_part, shared_up_part):
    gate_part = jnp.einsum(
        "secd,edf->secf", buffer, expert_gate, preferred_element_type=jnp.float32
    )
    up_part = jnp.einsum("secd,edf->secf", buffer, expert_up, preferred_element_type=jnp.float32)
    gate_act, up_act, shared_gate_act, shared_up_act = lax.psum(
        (gate_part, up_part, shared_gate_part, shared_up_part), "tp"
    )
    hidden = (jax.nn.silu(gate_act) * up_act).astype(jnp.bfloat16)
    shared_hidden = (jax.nn.silu(shared_gate_act) * shared_up_act).astype(jnp.bfloat16)
    results = jnp.einsum(
        "secf,efd->secd", hidden, expert_down, preferred_element_type=jnp.float32
    ).astype(jnp.bfloat16)
    return (results, shared_hidden)


def on_device(
    tokens,
    routes,
    gates,
    pre_gain,
    expert_gate,
    expert_up,
    expert_down,
    shared_gate,
    shared_up,
    shared_down,
    out_gain,
):
    own_rows = tokens.astype(jnp.float32)
    in_squares = lax.psum(jnp.sum(own_rows * own_rows, axis=1), "tp")
    normed = normalize(own_rows, pre_gain, in_squares, D).astype(jnp.bfloat16)
    shared_gate_part = jnp.dot(normed, shared_gate, preferred_element_type=jnp.float32)
    shared_up_part = jnp.dot(normed, shared_up, preferred_element_type=jnp.float32)
    tok_count = tokens.shape[0]
    top_count = routes.shape[1]
    groups = lax.axis_size("ep")
    local_experts = expert_gate.shape[0]
    experts_all = local_experts * groups
    capacity = max(2, 3 * tok_count * top_count // (2 * experts_all))
    places = jnp.arange(capacity, dtype=jnp.int32)
    zero_value = jnp.zeros((), jnp.float32)
    labels = jnp.arange(experts_all, dtype=jnp.int32)
    picked = routes[:, :, None] == labels[None, None, :]
    onehot = jnp.sum(picked.astype(jnp.int32), axis=1)
    dense_gate = jnp.sum(jnp.where(picked, gates[:, :, None], zero_value), axis=1)
    slot_index = jnp.cumsum(onehot, axis=0) - onehot
    select = (slot_index.T[:, None, :] == places[None, :, None]) & (onehot.T[:, None, :] > 0)
    outgoing = jnp.einsum(
        "ect,td->ecd", select.astype(jnp.bfloat16), normed, preferred_element_type=jnp.float32
    ).astype(jnp.bfloat16)
    outgoing = outgoing.reshape(groups, local_experts, capacity, normed.shape[1])
    received = lax.all_to_all(outgoing, "ep", split_axis=0, concat_axis=0, tiled=True)
    results, shared_hidden = expert_apply(
        received, expert_gate, expert_up, expert_down, shared_gate_part, shared_up_part
    )
    returned = lax.all_to_all(results, "ep", split_axis=0, concat_axis=0, tiled=True)
    weight = jnp.where(select, dense_gate.T[:, None, :], zero_value)
    returned_rows = returned.reshape(experts_all, capacity, normed.shape[1]).astype(jnp.float32)
    routed = jnp.einsum("ect,ecd->td", weight, returned_rows, precision=lax.Precision.HIGHEST)
    shared_out = jnp.dot(shared_hidden, shared_down, preferred_element_type=jnp.float32)
    combined = routed + shared_out
    out_squares = lax.psum(jnp.sum(combined * combined, axis=1), "tp")
    return normalize(combined, out_gain, out_squares, D).astype(jnp.bfloat16)


F32 = jnp.float32
BF16 = jnp.bfloat16
LANES = 128


def flip(index, mask):
    out, bit = index, 1
    while bit <= mask:
        if mask & bit:
            out = out + bit - 2 * bit * ((index // bit) % 2)
        bit *= 2
    return out


def iota(shape, dim):
    return lax.broadcasted_iota(jnp.int32, shape, dim)


def dot(a, b):
    return jnp.dot(a, b, preferred_element_type=F32)


def batches(n_ep):
    far = list(range(2, n_ep, 2))
    return [[0] + far[:-2], far[-2:-1], far[-1:]]


def fused_kernel(
    n_ep, n_tp, cap, width,
    tok_hbm, routes_hbm, gates_hbm, pre_hbm, eg_hbm, eu_hbm, ed_hbm, sg_hbm, su_hbm, sd_hbm, outg_hbm,
    o_ref,
    tok_ref, routes_ref, gates_ref, pre_ref, outg_ref,
    wg, wu, wd, sg, su, sd,
    xall, ss_all, bufs,
    rs_send, rs_recv, rs_own, rsh_send, rsh_recv, rsh_own,
    hid, hidsh, yown, yhold, ysend, ypair, zsend, zrecv, sq_all,
    w_sem, x_send, x_recv, ss_send, ss_recv, rs_ssem, rs_rsem, rsh_ssem, rsh_rsem,
    h_ssem, h_rsem, hs_ssem, hs_rsem, p_ssem, p_rsem, y_ssem, y_rsem, q_ssem, q_rsem,
):
    me = lax.axis_index("ep")
    mine = lax.axis_index("tp")
    tok, dim = tok_ref.shape
    local = eg_hbm.shape[0]
    experts = local * n_ep
    top = routes_hbm.shape[0]
    part = eg_hbm.shape[2] // n_tp
    tp_masks = sorted(range(1, n_tp), key=lambda m: -bin(m).count("1"))
    evens = batches(n_ep)
    count = len(evens)
    order = [m for batch in evens for m in batch + [m + 1 for m in batch]]
    place = {m: i for i, m in enumerate(order)}
    owner = {m: b for b, batch in enumerate(evens) for m in batch}
    far = [m for batch in evens for m in batch if m]
    slot = {m: i for i, m in enumerate(far)}
    pairs = [len(batch) for batch in evens]
    start = [place[batch[0]] for batch in evens]
    span = [2 * p * tok for p in pairs]
    per = [2 * p * cap for p in pairs]
    rows = [local * p for p in per]

    def at_ep(mask):
        return {"ep": flip(me, mask)}

    def at_tp(mask):
        return {"tp": flip(mine, mask)}

    barrier = pltpu.get_barrier_semaphore()
    for m in far + [1]:
        pl.semaphore_signal(barrier, inc=1, device_id=at_ep(m), device_id_type=pl.DeviceIdType.MESH)
    for m in range(1, n_tp):
        pl.semaphore_signal(barrier, inc=1, device_id=at_tp(m), device_id_type=pl.DeviceIdType.MESH)

    copies = {}
    loads = (
        ("routes", routes_hbm, routes_ref), ("gates", gates_hbm, gates_ref), ("tok", tok_hbm, tok_ref),
        ("pre", pre_hbm, pre_ref), ("sg", sg_hbm, sg), ("su", su_hbm, su), ("g", eg_hbm, wg), ("u", eu_hbm, wu),
        ("sd", sd_hbm, sd), ("d", ed_hbm, wd), ("outg", outg_hbm, outg_ref),
    )
    for i, (name, src, dst) in enumerate(loads):
        copies[name] = pltpu.make_async_copy(src, dst, w_sem.at[i])
        copies[name].start()

    def describe(src, dst, ssem, rsem, where):
        return pltpu.make_async_remote_copy(
            src_ref=src, dst_ref=dst, send_sem=ssem, recv_sem=rsem,
            device_id=where, device_id_type=pl.DeviceIdType.MESH,
        )

    def send(src, dst, ssem, rsem, where):
        describe(src, dst, ssem, rsem, where).start()

    def arrived(ref, ssem, rsem, where):
        describe(ref, ref, ssem, rsem, where).wait_recv()

    def sent(ref, ssem, rsem, where):
        describe(ref, ref, ssem, rsem, where).wait_send()

    def flat_gain(ref):
        value = ref[...].astype(F32)
        return jnp.concatenate([value[i : i + 1, :] for i in range(ref.shape[0])], axis=1)

    ss_all[:, 0] = jnp.zeros((ss_all.shape[0],) + ss_all.shape[2:], F32)
    copies["routes"].wait()
    copies["gates"].wait()
    row = iota((LANES, tok), 0)
    names = row % experts
    dense = jnp.zeros((LANES, tok), F32)
    for k in range(top):
        dense = dense + jnp.where(routes_ref[k : k + 1, :] == names, gates_ref[k : k + 1, :], 0.0)
    earlier = jnp.where(iota((tok, tok), 0) < iota((tok, tok), 1), 1.0, 0.0).astype(BF16)
    slots = dot(jnp.where(dense > 0.0, 1.0, 0.0).astype(BF16), earlier)
    slots = jnp.where(dense > 0.0, slots + 1.0, 0.0)

    def terms(value):
        hi = value.astype(BF16).astype(F32)
        mid = (value - hi).astype(BF16).astype(F32)
        return hi, mid, value - hi - mid

    def choose(index, values):
        out = 0.0
        for i, value in enumerate(values):
            out = jnp.where(index == i, value, out)
        return out

    listed = choose(row // experts, terms(dense) + (slots,)).astype(BF16)
    eye = jnp.where(iota((tok, tok), 0) == iota((tok, tok), 1), 1.0, 0.0).astype(BF16)
    meta = lax.dot_general(eye, listed, (((1,), (1,)), ((), ())), preferred_element_type=F32)
    copies["tok"].wait()
    copies["pre"].wait()
    x = tok_ref[...].astype(F32)
    xall[0, :, :dim] = (x * flat_gain(pre_ref)).astype(BF16)
    squares = jnp.sum(x * x, axis=1, keepdims=True)
    lane = iota((tok, LANES), 1)
    meta = jnp.where(lane < 4 * experts, meta, choose(lane - 4 * experts, terms(squares)))
    xall[0, :, dim:] = meta.astype(BF16)

    pl.semaphore_wait(barrier, len(far) + 1 + n_tp - 1)

    def x_to(m, held, put, index):
        send(xall.at[held], xall.at[put], x_send.at[0], x_recv.at[index], at_ep(m))

    odd = len(far)
    x_to(1, 0, place[1], odd)
    for m in far:
        x_to(m, 0, place[m], slot[m])

    def relay(m):
        arrived(xall.at[place[m]], x_send.at[0], x_recv.at[slot[m]], at_ep(m))
        x_to(1, place[m], place[m + 1], odd + owner[m])

    def columns(m):
        return pl.ds(pl.multiple_of(flip(mine, m) * part, part), part)

    xs = xall[0, :, :dim]
    def shared_pieces():
      copies["sg"].wait()
      copies["su"].wait()
      for m in tp_masks + [0]:
        g = dot(xs, sg[:, columns(m)])
        u = dot(xs, su[:, columns(m)])
        if m:
            rsh_send[m - 1, :, :part] = g.astype(BF16)
            rsh_send[m - 1, :, part:] = u.astype(BF16)
            send(rsh_send.at[m - 1], rsh_recv.at[m - 1], rsh_ssem.at[0], rsh_rsem.at[0], at_tp(m))
        else:
            rsh_own[:, :part] = g
            rsh_own[:, part:] = u

    shared_pieces()

    def odds(b):
        return xall.at[pl.ds(start[b] + pairs[b], pairs[b])]

    row8, lane8 = iota((8, LANES), 0), iota((8, LANES), 1)
    gate_lane = lane8 < 3 * experts
    slot_lane = (lane8 >= 3 * experts) & (lane8 < 4 * experts)
    mine8 = me * local + row8
    pick = (
        ((row8 < local) & gate_lane & (lane8 % experts == mine8))
        | ((row8 == local) & (lane8 >= 4 * experts))
        | ((row8 > local) & (row8 <= 2 * local) & slot_lane & (lane8 % experts == mine8 - local - 1))
    )
    pick = jnp.where(pick, 1.0, 0.0).astype(BF16)
    tables, chosen, scale, own = {}, {}, {}, {}

    def gather(b):
        arrived(odds(b), x_send.at[0], x_recv.at[odd + b], at_ep(1))
        blocks = pl.ds(start[b], 2 * pairs[b])
        tail = xall[blocks, :, dim:].reshape(span[b], LANES)
        table = lax.dot_general(pick, tail, (((1,), (1,)), ((), ())), preferred_element_type=F32)
        ss_all[b, 0, :, : span[b]] = table[local : local + 1, :]
        for m in tp_masks:
            send(ss_all.at[b, 0], ss_all.at[b, m], ss_send.at[0], ss_recv.at[b], at_tp(m))
        first = (iota((8, span[b]), 1) // tok) * cap - 1
        target = jnp.where(table > 0.5, first + table.astype(jnp.int32), -rows[b])
        pieces = [
            jnp.where(iota((rows[b], span[b]), 0) == target[local + 1 + e : local + 2 + e, :] + e * per[b], 1.0, 0.0)
            for e in range(local)
        ]
        tables[b], chosen[b] = table, pieces
        flat = xall[blocks, :, :dim].reshape(span[b], dim)
        for e in range(local):
            bufs[b][e] = dot(pieces[e].astype(BF16), flat).astype(BF16)

    def piece(b, m):
        g, u = 0.0, 0.0
        for e in range(local):
            rhs = bufs[b][e]
            g = g + dot(rhs, wg[e, :, columns(m)])
            u = u + dot(rhs, wu[e, :, columns(m)])
        if m:
            rs_send[b][m - 1, :, :part] = g.astype(BF16)
            rs_send[b][m - 1, :, part:] = u.astype(BF16)
            send(rs_send[b].at[m - 1], rs_recv[b].at[m - 1], rs_ssem.at[b], rs_rsem.at[b], at_tp(m))
        else:
            rs_own[b][:, :part] = g
            rs_own[b][:, part:] = u

    def scales(b):
        arrived(ss_all.at[b, pl.ds(1, n_tp - 1)], ss_send.at[0], ss_recv.at[b], at_tp(1))
        ss = ss_all[b, 0, :, : span[b]]
        for m in range(1, n_tp):
            ss = ss + ss_all[b, m, :, : span[b]]
        scale[b] = lax.rsqrt(ss / width + 1e-06)

    def activate(sums, by):
        g, u = sums[:, :part] * by, sums[:, part:] * by
        return (g / (1.0 + jnp.exp(-g)) * u).astype(BF16)

    def act(b):
        by = jnp.sum(sum(chosen[b]) * scale[b], axis=1, keepdims=True)
        arrived(rs_recv[b], rs_ssem.at[b], rs_rsem.at[b], at_tp(1))
        sums = rs_own[b][...]
        for m in tp_masks:
            sums = sums + rs_recv[b][m - 1].astype(F32)
        hid[b][0] = activate(sums, by)
        for m in tp_masks:
            send(hid[b].at[0], hid[b].at[m], h_ssem.at[b], h_rsem.at[b], at_tp(m))

    def down(b, m, e):
        depth = pl.ds(pl.multiple_of(flip(mine, m) * part, part), part)
        return dot(hid[b][m], wd[e, depth, :])

    def down_own(b):
        own[b] = [down(b, 0, e) for e in range(local)]

    def ypart(b):
        return pl.ds(start[b] // 2, pairs[b])

    def back(b):
        arrived(hid[b].at[pl.ds(1, n_tp - 1)], h_ssem.at[b], h_rsem.at[b], at_tp(1))
        gated = 0.0
        for e in range(local):
            acc = own[b][e]
            for m in tp_masks[::-1]:
                acc = acc + down(b, m, e)
            gated = gated + acc * jnp.sum(chosen[b][e] * tables[b][e : e + 1, :], axis=1, keepdims=True)
        y = lax.dot_general(
            sum(chosen[b]).astype(BF16), gated.astype(BF16), (((0,), (0,)), ((), ())), preferred_element_type=F32
        ).reshape(2 * pairs[b], tok, dim)
        ysend[ypart(b)] = y[pairs[b] :].astype(BF16)
        yhold[ypart(b)] = y[: pairs[b]]
        send(ysend.at[ypart(b)], ypair.at[ypart(b)], p_ssem.at[0], p_rsem.at[b], at_ep(1))

    def forward(b):
        arrived(ypair.at[ypart(b)], p_ssem.at[0], p_rsem.at[b], at_ep(1))
        for i, m in enumerate(evens[b]):
            both = yhold[start[b] // 2 + i] + ypair[start[b] // 2 + i].astype(F32)
            if m:
                zsend[slot[m]] = both.astype(BF16)
                send(zsend.at[slot[m]], zrecv.at[slot[m]], y_ssem.at[0], y_rsem.at[b], at_ep(m))
            else:
                kept.append(both)

    def shared_act():
        match = jnp.where(iota((tok, span[0]), 1) == iota((tok, span[0]), 0), 1.0, 0.0)
        by = jnp.sum(match * scale[0], axis=1, keepdims=True)
        arrived(rsh_recv, rsh_ssem.at[0], rsh_rsem.at[0], at_tp(1))
        sums = rsh_own[...]
        for m in tp_masks:
            sums = sums + rsh_recv[m - 1].astype(F32)
        hidsh[0] = activate(sums, by)
        for m in tp_masks:
            send(hidsh.at[0], hidsh.at[m], hs_ssem.at[0], hs_rsem.at[0], at_tp(m))

    def shared_down():
        arrived(hidsh.at[pl.ds(1, n_tp - 1)], hs_ssem.at[0], hs_rsem.at[0], at_tp(1))
        shared_out = 0.0
        for m in range(n_tp):
            depth = pl.ds(pl.multiple_of(flip(mine, m) * part, part), part)
            shared_out = shared_out + dot(hidsh[m], sd[depth, :])
        yown[...] = shared_out

    kept = []
    for m in evens[0][1:]:
        relay(m)
    gather(0)
    copies["g"].wait()
    copies["u"].wait()
    piece(0, tp_masks[0])
    for m in evens[1]:
        relay(m)
    for m in tp_masks[1:] + [0]:
        piece(0, m)
    gather(1)
    for m in evens[2]:
        relay(m)
    for m in tp_masks:
        piece(1, m)
    gather(2)
    for m in tp_masks:
        piece(2, m)
    scales(0)
    act(0)
    shared_act()
    piece(1, 0)
    scales(1)
    act(1)
    piece(2, 0)
    copies["d"].wait()
    copies["sd"].wait()
    down_own(0)
    down_own(1)
    scales(2)
    act(2)
    back(0)
    shared_down()
    back(1)
    forward(0)
    down_own(2)
    back(2)
    forward(1)
    forward(2)
    combined = yown[...]
    for both in kept:
        combined = combined + both
    copies["outg"].wait()
    for b, batch in enumerate(evens):
        held = [slot[m] for m in batch if m]
        if held:
            arrived(zrecv.at[pl.ds(held[0], len(held))], y_ssem.at[0], y_rsem.at[b], at_ep(2))
            for i in held:
                combined = combined + zrecv[i].astype(F32)

    squared = combined * combined
    lanes = squared[:, :LANES]
    for c in range(LANES, dim, LANES):
        lanes = lanes + squared[:, c : c + LANES]
    sq_all[0] = lanes
    for m in tp_masks:
        send(sq_all.at[0], sq_all.at[m], q_ssem.at[0], q_rsem.at[0], at_tp(m))
    scaled = combined * flat_gain(outg_ref)
    arrived(sq_all.at[pl.ds(1, n_tp - 1)], q_ssem.at[0], q_rsem.at[0], at_tp(1))
    lanes = sq_all[0]
    for m in range(1, n_tp):
        lanes = lanes + sq_all[m]
    mean = jnp.sum(lanes, axis=1, keepdims=True) / width
    o_ref[...] = (scaled * lax.rsqrt(mean + 1e-06)).astype(BF16)
    sent(xall.at[pl.ds(0, n_ep - 1)], x_send.at[0], x_recv.at[0], at_ep(1))
    sent(ss_all.at[:, pl.ds(1, n_tp - 1)], ss_send.at[0], ss_recv.at[0], at_tp(1))
    sent(rsh_send, rsh_ssem.at[0], rsh_rsem.at[0], at_tp(1))
    for b in range(count):
        sent(rs_send[b], rs_ssem.at[b], rs_rsem.at[b], at_tp(1))
        sent(hid[b].at[pl.ds(1, n_tp - 1)], h_ssem.at[b], h_rsem.at[b], at_tp(1))
    sent(hidsh.at[pl.ds(1, n_tp - 1)], hs_ssem.at[0], hs_rsem.at[0], at_tp(1))
    sent(ysend, p_ssem.at[0], p_rsem.at[0], at_ep(1))
    sent(zsend, y_ssem.at[0], y_rsem.at[0], at_ep(2))
    sent(sq_all.at[pl.ds(1, n_tp - 1)], q_ssem.at[0], q_rsem.at[0], at_tp(1))


def fused(n_ep, n_tp, tokens, routes, gates, pre_gain, eg, eu, ed, sg, su, sd, out_gain):
    tok, dim = tokens.shape
    local, _, hidden = eg.shape
    top = routes.shape[1]
    cap = max(2, 3 * tok * top // (2 * local * n_ep))
    half = n_ep // 2
    evens = batches(n_ep)
    count = len(evens)
    rows = [local * 2 * len(batch) * cap for batch in evens]
    part = hidden // n_tp
    anywhere = pl.BlockSpec(memory_space=pl.ANY)
    sems = lambda n: pltpu.SemaphoreType.DMA((n,))
    return pl.pallas_call(
        functools.partial(fused_kernel, n_ep, n_tp, cap, dim * n_tp),
        out_shape=pltpu.VMEM((tok, dim), BF16),
        in_specs=[anywhere] * 11,
        out_specs=pl.BlockSpec(memory_space=pltpu.VMEM),
        scratch_shapes=[
            pltpu.VMEM((tok, dim), BF16), pltpu.VMEM((top, tok), jnp.int32), pltpu.VMEM((top, tok), F32),
            pltpu.VMEM((dim // LANES, LANES), BF16), pltpu.VMEM((dim // LANES, LANES), BF16),
            pltpu.VMEM(eg.shape, BF16), pltpu.VMEM(eu.shape, BF16), pltpu.VMEM(ed.shape, BF16),
            pltpu.VMEM(sg.shape, BF16), pltpu.VMEM(su.shape, BF16), pltpu.VMEM(sd.shape, BF16),
            pltpu.VMEM((n_ep, tok, dim + LANES), BF16),
            pltpu.VMEM((count, n_tp, 1, LANES), F32),
            [pltpu.VMEM((local, r, dim), BF16) for r in rows],
            [pltpu.VMEM((n_tp - 1, r, 2 * part), BF16) for r in rows],
            [pltpu.VMEM((n_tp - 1, r, 2 * part), BF16) for r in rows],
            [pltpu.VMEM((r, 2 * part), F32) for r in rows],
            pltpu.VMEM((n_tp - 1, tok, 2 * part), BF16),
            pltpu.VMEM((n_tp - 1, tok, 2 * part), BF16),
            pltpu.VMEM((tok, 2 * part), F32),
            [pltpu.VMEM((n_tp, r, part), BF16) for r in rows],
            pltpu.VMEM((n_tp, tok, part), BF16),
            pltpu.VMEM((tok, dim), F32),
            pltpu.VMEM((half, tok, dim), F32),
            pltpu.VMEM((half, tok, dim), BF16),
            pltpu.VMEM((half, tok, dim), BF16),
            pltpu.VMEM((half - 1, tok, dim), BF16),
            pltpu.VMEM((half - 1, tok, dim), BF16),
            pltpu.VMEM((n_tp, tok, LANES), F32),
            sems(11),
            sems(1), sems(half - 1 + count), sems(1), sems(count), sems(count), sems(count), sems(1), sems(1),
            sems(count), sems(count), sems(1), sems(1), sems(1), sems(count), sems(1), sems(count), sems(1), sems(1),
        ],
        compiler_params=pltpu.CompilerParams(
            collective_id=0, has_side_effects=True, vmem_limit_bytes=60 * 1024 * 1024
        ),
    )(
        tokens, routes.T, gates.T, pre_gain.reshape(-1, LANES), eg, eu, ed, sg, su, sd,
        out_gain.reshape(-1, LANES),
    )


def fits(n_ep, n_tp, tokens, routes, eg):
    tok, dim = tokens.shape
    local, _, hidden = eg.shape
    experts = local * n_ep
    cap = max(2, 3 * tok * routes.shape[1] // (2 * experts))
    power = (n_ep & (n_ep - 1)) == 0 and (n_tp & (n_tp - 1)) == 0
    return (
        power
        and n_ep > 4
        and n_tp > 1
        and hidden % (LANES * n_tp) == 0
        and dim % LANES == 0
        and tok % 16 == 0
        and n_ep * tok == LANES
        and 4 * experts + 3 <= LANES
        and 2 * local < 8
    )


def per_device(*args):
    n_ep, n_tp = lax.axis_size("ep"), lax.axis_size("tp")
    if fits(n_ep, n_tp, args[0], args[1], args[4]):
        return fused(n_ep, n_tp, *args)
    return on_device(*args)


def solution(mesh):
    in_specs = (
        P("ep", "tp"),
        P("ep", None),
        P("ep", None),
        P("tp"),
        P("ep", "tp", None),
        P("ep", "tp", None),
        P("ep", None, "tp"),
        P("tp", None),
        P("tp", None),
        P(None, "tp"),
        P("tp"),
    )
    out_specs = P("ep", "tp")
    return jax.shard_map(
        per_device, mesh=mesh, in_specs=in_specs, out_specs=out_specs, check_vma=False
    )
```

time: 33.5 us -> 31.5 us (0.940)
  Pallas kernels: 32.7 us -> 30.7 us
    pallas_call x1, Pallas kernels: 32.7 us -> 30.7 us  [fused(): pl.pallas_call(functools.partial(fused_kernel, n_ep, n_tp, cap, dim * n_t...]
where the time goes in v2:
time: 31.5 us; the launch traced here: 31.4 us
  Pallas kernels  30.7 us (97%)
  local copies, waits for them, and re-layouts  0.62 us (2%)
    pallas_call x1, Pallas kernels, fused(): pl.pallas_call(functools.partial(fused_kernel, n_ep, n_tp, cap, dim * n_t...  30.7 us

profile of v2, /device:TPU:0, one launch (start us, length us, event | category | flops | bytes accessed | tf_op | source)
XLA Modules:
  0.0 31.4 jit_solution(1371418392286590299)
XLA Ops:
  0.0 30.7 %shard_map.109 = bf16[16,1024]{1,0:T(8,128)(2,1)S(1)} custom-call(bf16[16,1024]{1,0:T(8,128)(2,1)} %tok_hbm.1, s32[4,16]{1,0:T(4,128)} %bitcast.4, f32[4,16]{1,0:T(4,128)} %bitcast.5, bf16[8,128]{1,0:T(8,128)(2,1)} %bitcast.6, bf16[2,1024,1024]{2,1,0:T(8,128)(2,1)} %eg_hbm.1, bf16[2,1024,1024]{2,1,0:T(8,128)(2,1)} %eu_hbm.1, bf16[2,1024,1024]{2,1,0:T(8,128)(2,1)} %ed_hbm.1, ...), custom_call_target="tpu_custom_call" | custom-call | tf_op jit(solution)/shard_map/pallas_call | solution.py:465
  30.7 0.6 %copy.13 = bf16[16,1024]{1,0:T(8,128)(2,1)} copy(bf16[16,1024]{1,0:T(8,128)(2,1)S(1)} %shard_map.109) | data formatting | bytes 65536

commit v3 on v2

--- a/solution.py
+++ b/solution.py
@@ -104,7 +104,7 @@
 
 def batches(n_ep):
     far = list(range(2, n_ep, 2))
-    return [[0] + far[:-2], far[-2:-1], far[-1:]]
+    return [[0], far[-2::-1], far[-1:]]
 
 
 def fused_kernel(
@@ -114,8 +114,8 @@
     tok_ref, routes_ref, gates_ref, pre_ref, outg_ref,
     wg, wu, wd, sg, su, sd,
     xall, ss_all, bufs,
-    rs_send, rs_recv, rs_own, rsh_send, rsh_recv, rsh_own,
-    hid, hidsh, yown, yhold, ysend, ypair, zsend, zrecv, sq_all,
+    rs_send, rs_recv, rsh_send, rsh_recv, rsh_own,
+    hid_out, hid, hidsh, yown, yhold, ysend, ypair, zsend, zrecv, sq_all,
     w_sem, x_send, x_recv, ss_send, ss_recv, rs_ssem, rs_rsem, rsh_ssem, rsh_rsem,
     h_ssem, h_rsem, hs_ssem, hs_rsem, p_ssem, p_rsem, y_ssem, y_rsem, q_ssem, q_rsem,
 ):
@@ -146,21 +146,33 @@
     def at_tp(mask):
         return {"tp": flip(mine, mask)}
 
+    def across(mask):
+        return {"ep": flip(me, 1), "tp": flip(mine, mask)}
+
     barrier = pltpu.get_barrier_semaphore()
-    for m in far + [1]:
-        pl.semaphore_signal(barrier, inc=1, device_id=at_ep(m), device_id_type=pl.DeviceIdType.MESH)
-    for m in range(1, n_tp):
-        pl.semaphore_signal(barrier, inc=1, device_id=at_tp(m), device_id_type=pl.DeviceIdType.MESH)
+    peers = [at_ep(m + 1) for m in [0] + far]
+    peers += [where(m) for m in range(1, n_tp) for where in (at_tp, across)]
+    for where in peers:
+        pl.semaphore_signal(barrier, inc=1, device_id=where, device_id_type=pl.DeviceIdType.MESH)
+
+    def columns(m):
+        return pl.ds(pl.multiple_of(flip(mine, m) * part, part), part)
 
     copies = {}
     loads = (
         ("routes", routes_hbm, routes_ref), ("gates", gates_hbm, gates_ref), ("tok", tok_hbm, tok_ref),
-        ("pre", pre_hbm, pre_ref), ("sg", sg_hbm, sg), ("su", su_hbm, su), ("g", eg_hbm, wg), ("u", eu_hbm, wu),
-        ("sd", sd_hbm, sd), ("d", ed_hbm, wd), ("outg", outg_hbm, outg_ref),
+        ("pre", pre_hbm, pre_ref),
+    )
+    for m in tp_masks + [0]:
+        here = (slice(None), slice(None), columns(m))
+        loads += ((("g", m), eg_hbm.at[here], wg.at[here]), (("u", m), eu_hbm.at[here], wu.at[here]))
+    loads += (
+        ("sg", sg_hbm, sg), ("su", su_hbm, su), ("sd", sd_hbm, sd), ("d", ed_hbm, wd), ("outg", outg_hbm, outg_ref),
     )
     for i, (name, src, dst) in enumerate(loads):
         copies[name] = pltpu.make_async_copy(src, dst, w_sem.at[i])
-        copies[name].start()
+        if name not in ("sd", "d", "outg"):
+            copies[name].start()
 
     def describe(src, dst, ssem, rsem, where):
         return pltpu.make_async_remote_copy(
@@ -216,28 +228,22 @@
     meta = jnp.where(lane < 4 * experts, meta, choose(lane - 4 * experts, terms(squares)))
     xall[0, :, dim:] = meta.astype(BF16)
 
-    pl.semaphore_wait(barrier, len(far) + 1 + n_tp - 1)
+    pl.semaphore_wait(barrier, len(peers))
 
     def x_to(m, held, put, index):
         send(xall.at[held], xall.at[put], x_send.at[0], x_recv.at[index], at_ep(m))
 
     odd = len(far)
     x_to(1, 0, place[1], odd)
-    for m in far:
-        x_to(m, 0, place[m], slot[m])
+    for m in far[-2::-1] + far[-1:]:
+        x_to(m + 1, 0, place[m + 1], slot[m])
 
     def relay(m):
-        arrived(xall.at[place[m]], x_send.at[0], x_recv.at[slot[m]], at_ep(m))
-        x_to(1, place[m], place[m + 1], odd + owner[m])
-
-    def columns(m):
-        return pl.ds(pl.multiple_of(flip(mine, m) * part, part), part)
+        arrived(xall.at[place[m + 1]], x_send.at[0], x_recv.at[slot[m]], at_ep(m + 1))
+        x_to(1, place[m + 1], place[m], odd + owner[m])
 
     xs = xall[0, :, :dim]
-    def shared_pieces():
-      copies["sg"].wait()
-      copies["su"].wait()
-      for m in tp_masks + [0]:
+    def shared_piece(m):
         g = dot(xs, sg[:, columns(m)])
         u = dot(xs, su[:, columns(m)])
         if m:
@@ -248,55 +254,59 @@
             rsh_own[:, :part] = g
             rsh_own[:, part:] = u
 
-    shared_pieces()
-
-    def odds(b):
-        return xall.at[pl.ds(start[b] + pairs[b], pairs[b])]
+    def from_pair(b):
+        return xall.at[pl.ds(start[b] if b else place[1], pairs[b])]
 
     row8, lane8 = iota((8, LANES), 0), iota((8, LANES), 1)
     gate_lane = lane8 < 3 * experts
     slot_lane = (lane8 >= 3 * experts) & (lane8 < 4 * experts)
     mine8 = me * local + row8
+    pair8 = flip(me, 1) * local + row8
     pick = (
         ((row8 < local) & gate_lane & (lane8 % experts == mine8))
         | ((row8 == local) & (lane8 >= 4 * experts))
         | ((row8 > local) & (row8 <= 2 * local) & slot_lane & (lane8 % experts == mine8 - local - 1))
+        | ((row8 > 2 * local) & (row8 <= 3 * local) & slot_lane & (lane8 % experts == pair8 - 2 * local - 1))
     )
     pick = jnp.where(pick, 1.0, 0.0).astype(BF16)
-    tables, chosen, scale, own = {}, {}, {}, {}
+    tables, chosen, others, scale, own = {}, {}, {}, {}, {}
 
     def gather(b):
-        arrived(odds(b), x_send.at[0], x_recv.at[odd + b], at_ep(1))
+        arrived(from_pair(b), x_send.at[0], x_recv.at[odd + b], at_ep(1))
         blocks = pl.ds(start[b], 2 * pairs[b])
         tail = xall[blocks, :, dim:].reshape(span[b], LANES)
         table = lax.dot_general(pick, tail, (((1,), (1,)), ((), ())), preferred_element_type=F32)
         ss_all[b, 0, :, : span[b]] = table[local : local + 1, :]
         for m in tp_masks:
             send(ss_all.at[b, 0], ss_all.at[b, m], ss_send.at[0], ss_recv.at[b], at_tp(m))
-        first = (iota((8, span[b]), 1) // tok) * cap - 1
-        target = jnp.where(table > 0.5, first + table.astype(jnp.int32), -rows[b])
-        pieces = [
-            jnp.where(iota((rows[b], span[b]), 0) == target[local + 1 + e : local + 2 + e, :] + e * per[b], 1.0, 0.0)
-            for e in range(local)
-        ]
+        block = iota((8, span[b]), 1) // tok
+        seen = (block + pairs[b]) % (2 * pairs[b])
+        block = jnp.where(iota((8, span[b]), 0) > 2 * local, seen, block)
+        target = jnp.where(table > 0.5, block * cap - 1 + table.astype(jnp.int32), -rows[b])
+
+        def piece_of(e, base):
+            goal = target[base + e : base + e + 1, :] + e * per[b]
+            return jnp.where(iota((rows[b], span[b]), 0) == goal, 1.0, 0.0)
+
+        pieces = [piece_of(e, local + 1) for e in range(local)]
+        others[b] = sum(piece_of(e, 2 * local + 1) for e in range(local))
         tables[b], chosen[b] = table, pieces
         flat = xall[blocks, :, :dim].reshape(span[b], dim)
         for e in range(local):
             bufs[b][e] = dot(pieces[e].astype(BF16), flat).astype(BF16)
 
     def piece(b, m):
+        if b == 0:
+            copies["g", m].wait()
+            copies["u", m].wait()
         g, u = 0.0, 0.0
         for e in range(local):
             rhs = bufs[b][e]
             g = g + dot(rhs, wg[e, :, columns(m)])
             u = u + dot(rhs, wu[e, :, columns(m)])
-        if m:
-            rs_send[b][m - 1, :, :part] = g.astype(BF16)
-            rs_send[b][m - 1, :, part:] = u.astype(BF16)
-            send(rs_send[b].at[m - 1], rs_recv[b].at[m - 1], rs_ssem.at[b], rs_rsem.at[b], at_tp(m))
-        else:
-            rs_own[b][:, :part] = g
-            rs_own[b][:, part:] = u
+        rs_send[b][m, :, :part] = g.astype(BF16)
+        rs_send[b][m, :, part:] = u.astype(BF16)
+        send(rs_send[b].at[m], rs_recv[b].at[m], rs_ssem.at[b], rs_rsem.at[b], across(m))
 
     def scales(b):
         arrived(ss_all.at[b, pl.ds(1, n_tp - 1)], ss_send.at[0], ss_recv.at[b], at_tp(1))
@@ -310,27 +320,29 @@
         return (g / (1.0 + jnp.exp(-g)) * u).astype(BF16)
 
     def act(b):
-        by = jnp.sum(sum(chosen[b]) * scale[b], axis=1, keepdims=True)
-        arrived(rs_recv[b], rs_ssem.at[b], rs_rsem.at[b], at_tp(1))
-        sums = rs_own[b][...]
+        by = jnp.sum(others[b] * scale[b], axis=1, keepdims=True)
+        arrived(rs_recv[b], rs_ssem.at[b], rs_rsem.at[b], across(1))
+        sums = rs_recv[b][0].astype(F32)
         for m in tp_masks:
-            sums = sums + rs_recv[b][m - 1].astype(F32)
-        hid[b][0] = activate(sums, by)
+            sums = sums + rs_recv[b][m].astype(F32)
+        hid_out[b][...] = activate(sums, by)
         for m in tp_masks:
-            send(hid[b].at[0], hid[b].at[m], h_ssem.at[b], h_rsem.at[b], at_tp(m))
+            send(hid_out[b], hid[b].at[m], h_ssem.at[b], h_rsem.at[b], across(m))
+        send(hid_out[b], hid[b].at[0], h_ssem.at[b], h_rsem.at[count + b], at_ep(1))
 
     def down(b, m, e):
         depth = pl.ds(pl.multiple_of(flip(mine, m) * part, part), part)
         return dot(hid[b][m], wd[e, depth, :])
 
     def down_own(b):
+        arrived(hid[b].at[0], h_ssem.at[b], h_rsem.at[count + b], at_ep(1))
         own[b] = [down(b, 0, e) for e in range(local)]
 
     def ypart(b):
         return pl.ds(start[b] // 2, pairs[b])
 
     def back(b):
-        arrived(hid[b].at[pl.ds(1, n_tp - 1)], h_ssem.at[b], h_rsem.at[b], at_tp(1))
+        arrived(hid[b].at[pl.ds(1, n_tp - 1)], h_ssem.at[b], h_rsem.at[b], across(1))
         gated = 0.0
         for e in range(local):
             acc = own[b][e]
@@ -340,8 +352,9 @@
         y = lax.dot_general(
             sum(chosen[b]).astype(BF16), gated.astype(BF16), (((0,), (0,)), ((), ())), preferred_element_type=F32
         ).reshape(2 * pairs[b], tok, dim)
-        ysend[ypart(b)] = y[pairs[b] :].astype(BF16)
-        yhold[ypart(b)] = y[: pairs[b]]
+        even, uneven = y[: pairs[b]], y[pairs[b] :]
+        ysend[ypart(b)] = (even if b else uneven).astype(BF16)
+        yhold[ypart(b)] = uneven if b else even
         send(ysend.at[ypart(b)], ypair.at[ypart(b)], p_ssem.at[0], p_rsem.at[b], at_ep(1))
 
     def forward(b):
@@ -350,7 +363,7 @@
             both = yhold[start[b] // 2 + i] + ypair[start[b] // 2 + i].astype(F32)
             if m:
                 zsend[slot[m]] = both.astype(BF16)
-                send(zsend.at[slot[m]], zrecv.at[slot[m]], y_ssem.at[0], y_rsem.at[b], at_ep(m))
+                send(zsend.at[slot[m]], zrecv.at[slot[m]], y_ssem.at[0], y_rsem.at[b], at_ep(m + 1))
             else:
                 kept.append(both)
 
@@ -374,43 +387,45 @@
         yown[...] = shared_out
 
     kept = []
-    for m in evens[0][1:]:
-        relay(m)
     gather(0)
-    copies["g"].wait()
-    copies["u"].wait()
-    piece(0, tp_masks[0])
+    for name in ("sd", "d", "outg"):
+        copies[name].start()
+    for m in tp_masks + [0]:
+        piece(0, m)
     for m in evens[1]:
         relay(m)
-    for m in tp_masks[1:] + [0]:
-        piece(0, m)
+    copies["sg"].wait()
+    copies["su"].wait()
+    for m in tp_masks + [0]:
+        shared_piece(m)
     gather(1)
+    piece(1, tp_masks[0])
     for m in evens[2]:
         relay(m)
-    for m in tp_masks:
+    for m in tp_masks[1:]:
         piece(1, m)
+    scales(0)
+    act(0)
     gather(2)
     for m in tp_masks:
         piece(2, m)
-    scales(0)
-    act(0)
+    piece(1, 0)
+    piece(2, 0)
     shared_act()
-    piece(1, 0)
+    copies["d"].wait()
+    copies["sd"].wait()
     scales(1)
     act(1)
-    piece(2, 0)
-    copies["d"].wait()
-    copies["sd"].wait()
-    down_own(0)
-    down_own(1)
     scales(2)
     act(2)
+    down_own(0)
     back(0)
     shared_down()
+    down_own(1)
+    down_own(2)
     back(1)
+    back(2)
     forward(0)
-    down_own(2)
-    back(2)
     forward(1)
     forward(2)
     combined = yown[...]
@@ -420,7 +435,7 @@
     for b, batch in enumerate(evens):
         held = [slot[m] for m in batch if m]
         if held:
-            arrived(zrecv.at[pl.ds(held[0], len(held))], y_ssem.at[0], y_rsem.at[b], at_ep(2))
+            arrived(zrecv.at[pl.ds(held[0], len(held))], y_ssem.at[0], y_rsem.at[b], at_ep(3))
             for i in held:
                 combined = combined + zrecv[i].astype(F32)
 
@@ -442,11 +457,11 @@
     sent(ss_all.at[:, pl.ds(1, n_tp - 1)], ss_send.at[0], ss_recv.at[0], at_tp(1))
     sent(rsh_send, rsh_ssem.at[0], rsh_rsem.at[0], at_tp(1))
     for b in range(count):
-        sent(rs_send[b], rs_ssem.at[b], rs_rsem.at[b], at_tp(1))
-        sent(hid[b].at[pl.ds(1, n_tp - 1)], h_ssem.at[b], h_rsem.at[b], at_tp(1))
+        sent(rs_send[b], rs_ssem.at[b], rs_rsem.at[b], across(1))
+        sent(hid[b], h_ssem.at[b], h_rsem.at[b], across(1))
     sent(hidsh.at[pl.ds(1, n_tp - 1)], hs_ssem.at[0], hs_rsem.at[0], at_tp(1))
     sent(ysend, p_ssem.at[0], p_rsem.at[0], at_ep(1))
-    sent(zsend, y_ssem.at[0], y_rsem.at[0], at_ep(2))
+    sent(zsend, y_ssem.at[0], y_rsem.at[0], at_ep(3))
     sent(sq_all.at[pl.ds(1, n_tp - 1)], q_ssem.at[0], q_rsem.at[0], at_tp(1))
 
 
@@ -475,12 +490,12 @@
             pltpu.VMEM((n_ep, tok, dim + LANES), BF16),
             pltpu.VMEM((count, n_tp, 1, LANES), F32),
             [pltpu.VMEM((local, r, dim), BF16) for r in rows],
-            [pltpu.VMEM((n_tp - 1, r, 2 * part), BF16) for r in rows],
-            [pltpu.VMEM((n_tp - 1, r, 2 * part), BF16) for r in rows],
-            [pltpu.VMEM((r, 2 * part), F32) for r in rows],
+            [pltpu.VMEM((n_tp, r, 2 * part), BF16) for r in rows],
+            [pltpu.VMEM((n_tp, r, 2 * part), BF16) for r in rows],
             pltpu.VMEM((n_tp - 1, tok, 2 * part), BF16),
             pltpu.VMEM((n_tp - 1, tok, 2 * part), BF16),
             pltpu.VMEM((tok, 2 * part), F32),
+            [pltpu.VMEM((r, part), BF16) for r in rows],
             [pltpu.VMEM((n_tp, r, part), BF16) for r in rows],
             pltpu.VMEM((n_tp, tok, part), BF16),
             pltpu.VMEM((tok, dim), F32),
@@ -490,9 +505,9 @@
             pltpu.VMEM((half - 1, tok, dim), BF16),
             pltpu.VMEM((half - 1, tok, dim), BF16),
             pltpu.VMEM((n_tp, tok, LANES), F32),
-            sems(11),
+            sems(9 + 2 * n_tp),
             sems(1), sems(half - 1 + count), sems(1), sems(count), sems(count), sems(count), sems(1), sems(1),
-            sems(count), sems(count), sems(1), sems(1), sems(1), sems(count), sems(1), sems(count), sems(1), sems(1),
+            sems(count), sems(2 * count), sems(1), sems(1), sems(1), sems(count), sems(1), sems(count), sems(1), sems(1),
         ],
         compiler_params=pltpu.CompilerParams(
             collective_id=0, has_side_effects=True, vmem_limit_bytes=60 * 1024 * 1024
@@ -518,7 +533,7 @@
         and tok % 16 == 0
         and n_ep * tok == LANES
         and 4 * experts + 3 <= LANES
-        and 2 * local < 8
+        and 3 * local < 8
     )
 
 

time: 31.5 us -> 30.1 us (0.956)
  Pallas kernels: 30.7 us -> 29.4 us
    pallas_call x1, Pallas kernels: 30.7 us -> 29.4 us  [fused(): pl.pallas_call(functools.partial(fused_kernel, n_ep, n_tp, cap, dim * n_t...]
where the time goes in v3:
time: 30.1 us; the launch traced here: 30 us
  Pallas kernels  29.4 us (98%)
  local copies, waits for them, and re-layouts  0.62 us (2%)
    pallas_call x1, Pallas kernels, fused(): pl.pallas_call(functools.partial(fused_kernel, n_ep, n_tp, cap, dim * n_t...  29.4 us
    unnamed x1, local copies, waits for them, and re-layouts  0.62 us

profile of v3, /device:TPU:0, one launch (start us, length us, event | category | flops | bytes accessed | tf_op | source)
XLA Modules:
  0.0 30.0 jit_solution(17383942886694563416)
XLA Ops:
  0.0 29.4 %shard_map.109 = bf16[16,1024]{1,0:T(8,128)(2,1)S(1)} custom-call(bf16[16,1024]{1,0:T(8,128)(2,1)} %tok_hbm.1, s32[4,16]{1,0:T(4,128)} %bitcast.4, f32[4,16]{1,0:T(4,128)} %bitcast.5, bf16[8,128]{1,0:T(8,128)(2,1)} %bitcast.6, bf16[2,1024,1024]{2,1,0:T(8,128)(2,1)} %eg_hbm.1, bf16[2,1024,1024]{2,1,0:T(8,128)(2,1)} %eu_hbm.1, bf16[2,1024,1024]{2,1,0:T(8,128)(2,1)} %ed_hbm.1, ...), custom_call_target="tpu_custom_call" | custom-call | tf_op jit(solution)/shard_map/pallas_call | solution.py:480
  29.4 0.6 %copy.13 = bf16[16,1024]{1,0:T(8,128)(2,1)} copy(bf16[16,1024]{1,0:T(8,128)(2,1)S(1)} %shard_map.109) | data formatting | bytes 65536

commit v4 on v3

--- a/solution.py
+++ b/solution.py
@@ -116,8 +116,8 @@
     xall, ss_all, bufs,
     rs_send, rs_recv, rsh_send, rsh_recv, rsh_own,
     hid_out, hid, hidsh, yown, yhold, ysend, ypair, zsend, zrecv, sq_all,
-    w_sem, x_send, x_recv, ss_send, ss_recv, rs_ssem, rs_rsem, rsh_ssem, rsh_rsem,
-    h_ssem, h_rsem, hs_ssem, hs_rsem, p_ssem, p_rsem, y_ssem, y_rsem, q_ssem, q_rsem,
+    w_sem, x_send, x_recv, ss_send, ss_recv, rs_ssem, rs_rsem, rsh_rsem,
+    h_ssem, h_rsem, hs_rsem, p_ssem, p_rsem, y_rsem, q_ssem, q_rsem,
 ):
     me = lax.axis_index("ep")
     mine = lax.axis_index("tp")
@@ -194,8 +194,8 @@
         return jnp.concatenate([value[i : i + 1, :] for i in range(ref.shape[0])], axis=1)
 
     ss_all[:, 0] = jnp.zeros((ss_all.shape[0],) + ss_all.shape[2:], F32)
-    copies["routes"].wait()
-    copies["gates"].wait()
+    for name in ("routes", "gates", "tok", "pre"):
+        copies[name].wait()
     row = iota((LANES, tok), 0)
     names = row % experts
     dense = jnp.zeros((LANES, tok), F32)
@@ -219,8 +219,6 @@
     listed = choose(row // experts, terms(dense) + (slots,)).astype(BF16)
     eye = jnp.where(iota((tok, tok), 0) == iota((tok, tok), 1), 1.0, 0.0).astype(BF16)
     meta = lax.dot_general(eye, listed, (((1,), (1,)), ((), ())), preferred_element_type=F32)
-    copies["tok"].wait()
-    copies["pre"].wait()
     x = tok_ref[...].astype(F32)
     xall[0, :, :dim] = (x * flat_gain(pre_ref)).astype(BF16)
     squares = jnp.sum(x * x, axis=1, keepdims=True)
@@ -249,7 +247,7 @@
         if m:
             rsh_send[m - 1, :, :part] = g.astype(BF16)
             rsh_send[m - 1, :, part:] = u.astype(BF16)
-            send(rsh_send.at[m - 1], rsh_recv.at[m - 1], rsh_ssem.at[0], rsh_rsem.at[0], at_tp(m))
+            send(rsh_send.at[m - 1], rsh_recv.at[m - 1], rs_ssem.at[0], rsh_rsem.at[0], at_tp(m))
         else:
             rsh_own[:, :part] = g
             rsh_own[:, part:] = u
@@ -306,7 +304,7 @@
             u = u + dot(rhs, wu[e, :, columns(m)])
         rs_send[b][m, :, :part] = g.astype(BF16)
         rs_send[b][m, :, part:] = u.astype(BF16)
-        send(rs_send[b].at[m], rs_recv[b].at[m], rs_ssem.at[b], rs_rsem.at[b], across(m))
+        send(rs_send[b].at[m], rs_recv[b].at[m], rs_ssem.at[0], rs_rsem.at[b], across(m))
 
     def scales(b):
         arrived(ss_all.at[b, pl.ds(1, n_tp - 1)], ss_send.at[0], ss_recv.at[b], at_tp(1))
@@ -321,65 +319,75 @@
 
     def act(b):
         by = jnp.sum(others[b] * scale[b], axis=1, keepdims=True)
-        arrived(rs_recv[b], rs_ssem.at[b], rs_rsem.at[b], across(1))
+        arrived(rs_recv[b], rs_ssem.at[0], rs_rsem.at[b], across(1))
         sums = rs_recv[b][0].astype(F32)
         for m in tp_masks:
             sums = sums + rs_recv[b][m].astype(F32)
         hid_out[b][...] = activate(sums, by)
         for m in tp_masks:
-            send(hid_out[b], hid[b].at[m], h_ssem.at[b], h_rsem.at[b], across(m))
-        send(hid_out[b], hid[b].at[0], h_ssem.at[b], h_rsem.at[count + b], at_ep(1))
-
-    def down(b, m, e):
+            send(hid_out[b], hid[b].at[m], h_ssem.at[0], h_rsem.at[b * n_tp + m], across(m))
+        send(hid_out[b], hid[b].at[0], h_ssem.at[0], h_rsem.at[b * n_tp], at_ep(1))
+
+    def down(b, m, e, lo=0, hi=dim):
         depth = pl.ds(pl.multiple_of(flip(mine, m) * part, part), part)
-        return dot(hid[b][m], wd[e, depth, :])
+        return dot(hid[b][m], wd[e, depth, lo:hi])
 
     def down_own(b):
-        arrived(hid[b].at[0], h_ssem.at[b], h_rsem.at[count + b], at_ep(1))
+        arrived(hid[b].at[0], h_ssem.at[0], h_rsem.at[b * n_tp], at_ep(1))
         own[b] = [down(b, 0, e) for e in range(local)]
+
+    def down_near(b):
+        for m in tp_masks[1:]:
+            arrived(hid[b].at[m], h_ssem.at[0], h_rsem.at[b * n_tp + m], across(m))
+            own[b] = [own[b][e] + down(b, m, e) for e in range(local)]
 
     def ypart(b):
         return pl.ds(start[b] // 2, pairs[b])
 
-    def back(b):
-        arrived(hid[b].at[pl.ds(1, n_tp - 1)], h_ssem.at[b], h_rsem.at[b], across(1))
+    def back(b, lo=0, hi=dim, index=0):
+        m = tp_masks[0]
+        if lo == 0:
+            arrived(hid[b].at[m], h_ssem.at[0], h_rsem.at[b * n_tp + m], across(m))
         gated = 0.0
         for e in range(local):
-            acc = own[b][e]
-            for m in tp_masks[::-1]:
-                acc = acc + down(b, m, e)
+            acc = own[b][e][:, lo:hi] + down(b, m, e, lo, hi)
             gated = gated + acc * jnp.sum(chosen[b][e] * tables[b][e : e + 1, :], axis=1, keepdims=True)
         y = lax.dot_general(
             sum(chosen[b]).astype(BF16), gated.astype(BF16), (((0,), (0,)), ((), ())), preferred_element_type=F32
-        ).reshape(2 * pairs[b], tok, dim)
+        ).reshape(2 * pairs[b], tok, hi - lo)
         even, uneven = y[: pairs[b]], y[pairs[b] :]
-        ysend[ypart(b)] = (even if b else uneven).astype(BF16)
-        yhold[ypart(b)] = uneven if b else even
-        send(ysend.at[ypart(b)], ypair.at[ypart(b)], p_ssem.at[0], p_rsem.at[b], at_ep(1))
-
-    def forward(b):
-        arrived(ypair.at[ypart(b)], p_ssem.at[0], p_rsem.at[b], at_ep(1))
+        ysend[ypart(b), :, lo:hi] = (even if b else uneven).astype(BF16)
+        yhold[ypart(b), :, lo:hi] = uneven if b else even
+        block = (ypart(b), slice(None), pl.ds(lo, hi - lo))
+        send(ysend.at[block], ypair.at[block], p_ssem.at[0], p_rsem.at[index], at_ep(1))
+
+    def forward(b, lo=0, hi=dim, index=0):
+        if b:
+            block = (pl.ds(0, pairs[0] + pairs[1]) if b == 1 else ypart(b), slice(None), pl.ds(lo, hi - lo))
+            arrived(ypair.at[block], p_ssem.at[0], p_rsem.at[index], at_ep(1))
         for i, m in enumerate(evens[b]):
-            both = yhold[start[b] // 2 + i] + ypair[start[b] // 2 + i].astype(F32)
+            here = start[b] // 2 + i
+            both = yhold[here, :, lo:hi] + ypair[here, :, lo:hi].astype(F32)
             if m:
-                zsend[slot[m]] = both.astype(BF16)
-                send(zsend.at[slot[m]], zrecv.at[slot[m]], y_ssem.at[0], y_rsem.at[b], at_ep(m + 1))
+                zsend[slot[m], :, lo:hi] = both.astype(BF16)
+                block = (slot[m], slice(None), pl.ds(lo, hi - lo))
+                send(zsend.at[block], zrecv.at[block], p_ssem.at[0], y_rsem.at[0], at_ep(m + 1))
             else:
                 kept.append(both)
 
     def shared_act():
         match = jnp.where(iota((tok, span[0]), 1) == iota((tok, span[0]), 0), 1.0, 0.0)
         by = jnp.sum(match * scale[0], axis=1, keepdims=True)
-        arrived(rsh_recv, rsh_ssem.at[0], rsh_rsem.at[0], at_tp(1))
+        arrived(rsh_recv, rs_ssem.at[0], rsh_rsem.at[0], at_tp(1))
         sums = rsh_own[...]
         for m in tp_masks:
             sums = sums + rsh_recv[m - 1].astype(F32)
         hidsh[0] = activate(sums, by)
         for m in tp_masks:
-            send(hidsh.at[0], hidsh.at[m], hs_ssem.at[0], hs_rsem.at[0], at_tp(m))
+            send(hidsh.at[0], hidsh.at[m], h_ssem.at[0], hs_rsem.at[0], at_tp(m))
 
     def shared_down():
-        arrived(hidsh.at[pl.ds(1, n_tp - 1)], hs_ssem.at[0], hs_rsem.at[0], at_tp(1))
+        arrived(hidsh.at[pl.ds(1, n_tp - 1)], h_ssem.at[0], hs_rsem.at[0], at_tp(1))
         shared_out = 0.0
         for m in range(n_tp):
             depth = pl.ds(pl.multiple_of(flip(mine, m) * part, part), part)
@@ -419,25 +427,25 @@
     scales(2)
     act(2)
     down_own(0)
+    down_near(0)
     back(0)
     shared_down()
     down_own(1)
     down_own(2)
+    down_near(1)
     back(1)
-    back(2)
+    down_near(2)
+    back(2, 0, dim, 1)
+    forward(1)
+    forward(2, 0, dim, 1)
     forward(0)
-    forward(1)
-    forward(2)
     combined = yown[...]
     for both in kept:
         combined = combined + both
     copies["outg"].wait()
-    for b, batch in enumerate(evens):
-        held = [slot[m] for m in batch if m]
-        if held:
-            arrived(zrecv.at[pl.ds(held[0], len(held))], y_ssem.at[0], y_rsem.at[b], at_ep(3))
-            for i in held:
-                combined = combined + zrecv[i].astype(F32)
+    arrived(zrecv, p_ssem.at[0], y_rsem.at[0], at_ep(3))
+    for i in range(len(far)):
+        combined = combined + zrecv[i].astype(F32)
 
     squared = combined * combined
     lanes = squared[:, :LANES]
@@ -455,13 +463,10 @@
     o_ref[...] = (scaled * lax.rsqrt(mean + 1e-06)).astype(BF16)
     sent(xall.at[pl.ds(0, n_ep - 1)], x_send.at[0], x_recv.at[0], at_ep(1))
     sent(ss_all.at[:, pl.ds(1, n_tp - 1)], ss_send.at[0], ss_recv.at[0], at_tp(1))
-    sent(rsh_send, rsh_ssem.at[0], rsh_rsem.at[0], at_tp(1))
-    for b in range(count):
-        sent(rs_send[b], rs_ssem.at[b], rs_rsem.at[b], across(1))
-        sent(hid[b], h_ssem.at[b], h_rsem.at[b], across(1))
-    sent(hidsh.at[pl.ds(1, n_tp - 1)], hs_ssem.at[0], hs_rsem.at[0], at_tp(1))
-    sent(ysend, p_ssem.at[0], p_rsem.at[0], at_ep(1))
-    sent(zsend, y_ssem.at[0], y_rsem.at[0], at_ep(3))
+    lines = n_tp * sum(rows) + (n_tp - 1) * tok
+    sent(wd.at[0, pl.ds(0, lines), pl.ds(0, 2 * part)], rs_ssem.at[0], rs_rsem.at[0], across(1))
+    sent(wd.at[0, pl.ds(0, lines), pl.ds(0, part)], h_ssem.at[0], h_rsem.at[0], across(1))
+    sent(wd.at[0, pl.ds(0, (sum(pairs) + len(far)) * tok), :], p_ssem.at[0], p_rsem.at[0], at_ep(1))
     sent(sq_all.at[pl.ds(1, n_tp - 1)], q_ssem.at[0], q_rsem.at[0], at_tp(1))
 
 
@@ -506,8 +511,8 @@
             pltpu.VMEM((half - 1, tok, dim), BF16),
             pltpu.VMEM((n_tp, tok, LANES), F32),
             sems(9 + 2 * n_tp),
-            sems(1), sems(half - 1 + count), sems(1), sems(count), sems(count), sems(count), sems(1), sems(1),
-            sems(count), sems(2 * count), sems(1), sems(1), sems(1), sems(count), sems(1), sems(count), sems(1), sems(1),
+            sems(1), sems(half - 1 + count), sems(1), sems(count), sems(1), sems(count), sems(1),
+            sems(1), sems(n_tp * count), sems(1), sems(1), sems(3), sems(1), sems(1), sems(1),
         ],
         compiler_params=pltpu.CompilerParams(
             collective_id=0, has_side_effects=True, vmem_limit_bytes=60 * 1024 * 1024

time: 30.1 us -> 29.8 us (0.990)
    pallas_call x1, Pallas kernels: 29.4 us -> 29.1 us  [fused(): pl.pallas_call(functools.partial(fused_kernel, n_ep, n_tp, cap, dim * n_t...]
where the time goes in v4:
time: 29.8 us; the launch traced here: 29.7 us
  Pallas kernels  29.1 us (98%)
  local copies, waits for them, and re-layouts  0.62 us (2%)
    pallas_call x1, Pallas kernels, fused(): pl.pallas_call(functools.partial(fused_kernel, n_ep, n_tp, cap, dim * n_t...  29.1 us
    unnamed x1, local copies, waits for them, and re-layouts  0.62 us

profile of v4, /device:TPU:0, one launch (start us, length us, event | category | flops | bytes accessed | tf_op | source)
XLA Modules:
  0.0 29.7 jit_solution(11297899119043565367)
XLA Ops:
  0.0 29.1 %shard_map.109 = bf16[16,1024]{1,0:T(8,128)(2,1)S(1)} custom-call(bf16[16,1024]{1,0:T(8,128)(2,1)} %tok_hbm.1, s32[4,16]{1,0:T(4,128)} %bitcast.4, f32[4,16]{1,0:T(4,128)} %bitcast.5, bf16[8,128]{1,0:T(8,128)(2,1)} %bitcast.6, bf16[2,1024,1024]{2,1,0:T(8,128)(2,1)} %eg_hbm.1, bf16[2,1024,1024]{2,1,0:T(8,128)(2,1)} %eu_hbm.1, bf16[2,1024,1024]{2,1,0:T(8,128)(2,1)} %ed_hbm.1, ...), custom_call_target="tpu_custom_call" | custom-call | tf_op jit(solution)/shard_map/pallas_call | solution.py:485
  29.1 0.6 %copy.13 = bf16[16,1024]{1,0:T(8,128)(2,1)} copy(bf16[16,1024]{1,0:T(8,128)(2,1)S(1)} %shard_map.109) | data formatting | bytes 65536

commit v5 on v4

--- a/solution.py
+++ b/solution.py
@@ -201,9 +201,7 @@
     dense = jnp.zeros((LANES, tok), F32)
     for k in range(top):
         dense = dense + jnp.where(routes_ref[k : k + 1, :] == names, gates_ref[k : k + 1, :], 0.0)
-    earlier = jnp.where(iota((tok, tok), 0) < iota((tok, tok), 1), 1.0, 0.0).astype(BF16)
-    slots = dot(jnp.where(dense > 0.0, 1.0, 0.0).astype(BF16), earlier)
-    slots = jnp.where(dense > 0.0, slots + 1.0, 0.0)
+    named = jnp.where(dense > 0.0, 1.0, 0.0)
 
     def terms(value):
         hi = value.astype(BF16).astype(F32)
@@ -216,13 +214,20 @@
             out = jnp.where(index == i, value, out)
         return out
 
-    listed = choose(row // experts, terms(dense) + (slots,)).astype(BF16)
-    eye = jnp.where(iota((tok, tok), 0) == iota((tok, tok), 1), 1.0, 0.0).astype(BF16)
-    meta = lax.dot_general(eye, listed, (((1,), (1,)), ((), ())), preferred_element_type=F32)
+    def flipped(left, right):
+        return lax.dot_general(
+            jnp.where(left, 1.0, 0.0).astype(BF16), right.astype(BF16), (((1,), (1,)), ((), ())),
+            preferred_element_type=F32,
+        )
+
+    here, there = iota((tok, tok), 0), iota((tok, tok), 1)
+    meta = flipped(here == there, choose(row // experts, terms(dense) + (named,)))
+    before = flipped(there < here, named)
     x = tok_ref[...].astype(F32)
     xall[0, :, :dim] = (x * flat_gain(pre_ref)).astype(BF16)
     squares = jnp.sum(x * x, axis=1, keepdims=True)
     lane = iota((tok, LANES), 1)
+    meta = jnp.where(lane < 3 * experts, meta, meta * (before + 1.0))
     meta = jnp.where(lane < 4 * experts, meta, choose(lane - 4 * experts, terms(squares)))
     xall[0, :, dim:] = meta.astype(BF16)
 
@@ -317,6 +322,9 @@
         g, u = sums[:, :part] * by, sums[:, part:] * by
         return (g / (1.0 + jnp.exp(-g)) * u).astype(BF16)
 
+    def hidden_at(b, m):
+        return 1 + (b - 1) * n_tp + m if b else 0
+
     def act(b):
         by = jnp.sum(others[b] * scale[b], axis=1, keepdims=True)
         arrived(rs_recv[b], rs_ssem.at[0], rs_rsem.at[b], across(1))
@@ -325,20 +333,21 @@
             sums = sums + rs_recv[b][m].astype(F32)
         hid_out[b][...] = activate(sums, by)
         for m in tp_masks:
-            send(hid_out[b], hid[b].at[m], h_ssem.at[0], h_rsem.at[b * n_tp + m], across(m))
-        send(hid_out[b], hid[b].at[0], h_ssem.at[0], h_rsem.at[b * n_tp], at_ep(1))
+            send(hid_out[b], hid[b].at[m], h_ssem.at[0], h_rsem.at[hidden_at(b, m)], across(m))
+        send(hid_out[b], hid[b].at[0], h_ssem.at[0], h_rsem.at[hidden_at(b, 0)], at_ep(1))
 
     def down(b, m, e, lo=0, hi=dim):
         depth = pl.ds(pl.multiple_of(flip(mine, m) * part, part), part)
         return dot(hid[b][m], wd[e, depth, lo:hi])
 
     def down_own(b):
-        arrived(hid[b].at[0], h_ssem.at[0], h_rsem.at[b * n_tp], at_ep(1))
+        arrived(hid[b].at[0] if b else hid[b], h_ssem.at[0], h_rsem.at[hidden_at(b, 0)], at_ep(1))
         own[b] = [down(b, 0, e) for e in range(local)]
 
     def down_near(b):
         for m in tp_masks[1:]:
-            arrived(hid[b].at[m], h_ssem.at[0], h_rsem.at[b * n_tp + m], across(m))
+            if b:
+                arrived(hid[b].at[m], h_ssem.at[0], h_rsem.at[hidden_at(b, m)], across(m))
             own[b] = [own[b][e] + down(b, m, e) for e in range(local)]
 
     def ypart(b):
@@ -346,8 +355,8 @@
 
     def back(b, lo=0, hi=dim, index=0):
         m = tp_masks[0]
-        if lo == 0:
-            arrived(hid[b].at[m], h_ssem.at[0], h_rsem.at[b * n_tp + m], across(m))
+        if b and lo == 0:
+            arrived(hid[b].at[m], h_ssem.at[0], h_rsem.at[hidden_at(b, m)], across(m))
         gated = 0.0
         for e in range(local):
             acc = own[b][e][:, lo:hi] + down(b, m, e, lo, hi)
@@ -512,7 +521,7 @@
             pltpu.VMEM((n_tp, tok, LANES), F32),
             sems(9 + 2 * n_tp),
             sems(1), sems(half - 1 + count), sems(1), sems(count), sems(1), sems(count), sems(1),
-            sems(1), sems(n_tp * count), sems(1), sems(1), sems(3), sems(1), sems(1), sems(1),
+            sems(1), sems(1 + n_tp * (count - 1)), sems(1), sems(1), sems(2), sems(1), sems(1), sems(1),
         ],
         compiler_params=pltpu.CompilerParams(
             collective_id=0, has_side_effects=True, vmem_limit_bytes=60 * 1024 * 1024

time: 29.8 us -> 29.8 us (level)
  no operation moved by 1% of the time
where the time goes in v5:
time: 29.8 us; the launch traced here: 29.7 us
  Pallas kernels  29 us (97%)
  local copies, waits for them, and re-layouts  0.62 us (2%)
    pallas_call x1, Pallas kernels, fused(): pl.pallas_call(functools.partial(fused_kernel, n_ep, n_tp, cap, dim * n_t...  29 us
    unnamed x1, local copies, waits for them, and re-layouts  0.62 us

profile of v5, /device:TPU:0, one launch (start us, length us, event | category | flops | bytes accessed | tf_op | source)
XLA Modules:
  0.0 29.7 jit_solution(11653216117557080423)
XLA Ops:
  0.0 29.0 %shard_map.109 = bf16[16,1024]{1,0:T(8,128)(2,1)S(1)} custom-call(bf16[16,1024]{1,0:T(8,128)(2,1)} %tok_hbm.1, s32[4,16]{1,0:T(4,128)} %bitcast.4, f32[4,16]{1,0:T(4,128)} %bitcast.5, bf16[8,128]{1,0:T(8,128)(2,1)} %bitcast.6, bf16[2,1024,1024]{2,1,0:T(8,128)(2,1)} %eg_hbm.1, bf16[2,1024,1024]{2,1,0:T(8,128)(2,1)} %eu_hbm.1, bf16[2,1024,1024]{2,1,0:T(8,128)(2,1)} %ed_hbm.1, ...), custom_call_target="tpu_custom_call" | custom-call | tf_op jit(solution)/shard_map/pallas_call | solution.py:494
  29.0 0.6 %copy.13 = bf16[16,1024]{1,0:T(8,128)(2,1)} copy(bf16[16,1024]{1,0:T(8,128)(2,1)S(1)} %shard_map.109) | data formatting | bytes 65536

commit v6 on v5

--- a/solution.py
+++ b/solution.py
@@ -421,11 +421,11 @@
         relay(m)
     for m in tp_masks[1:]:
         piece(1, m)
-    scales(0)
-    act(0)
     gather(2)
     for m in tp_masks:
         piece(2, m)
+    scales(0)
+    act(0)
     piece(1, 0)
     piece(2, 0)
     shared_act()

time: 29.8 us -> 29.9 us (level)
  no operation moved by 1% of the time
where the time goes in v6:
time: 29.9 us; the launch traced here: 29.8 us
  Pallas kernels  29.2 us (98%)
  local copies, waits for them, and re-layouts  0.62 us (2%)
    pallas_call x1, Pallas kernels, fused(): pl.pallas_call(functools.partial(fused_kernel, n_ep, n_tp, cap, dim * n_t...  29.2 us
    unnamed x1, local copies, waits for them, and re-layouts  0.62 us

profile of v6, /device:TPU:0, one launch (start us, length us, event | category | flops | bytes accessed | tf_op | source)
XLA Modules:
  0.0 29.8 jit_solution(7301247802149485662)
XLA Ops:
  0.0 29.2 %shard_map.109 = bf16[16,1024]{1,0:T(8,128)(2,1)S(1)} custom-call(bf16[16,1024]{1,0:T(8,128)(2,1)} %tok_hbm.1, s32[4,16]{1,0:T(4,128)} %bitcast.4, f32[4,16]{1,0:T(4,128)} %bitcast.5, bf16[8,128]{1,0:T(8,128)(2,1)} %bitcast.6, bf16[2,1024,1024]{2,1,0:T(8,128)(2,1)} %eg_hbm.1, bf16[2,1024,1024]{2,1,0:T(8,128)(2,1)} %eu_hbm.1, bf16[2,1024,1024]{2,1,0:T(8,128)(2,1)} %ed_hbm.1, ...), custom_call_target="tpu_custom_call" | custom-call | tf_op jit(solution)/shard_map/pallas_call | solution.py:494
  29.2 0.6 %copy.13 = bf16[16,1024]{1,0:T(8,128)(2,1)} copy(bf16[16,1024]{1,0:T(8,128)(2,1)S(1)} %shard_map.109) | data formatting | bytes 65536
